TPU v7x, 1024 devices: a whole 4x4x32 slice. The times are simulated.
1024 devices in a mesh: fs: 256 (over z, x, core), tp: 4 (over y).
Axes of the slice: x: 4, y: 4, z: 32, core: 2. Of those that a mesh axis runs over, the one named last changes fastest.
Arguments:
- saved_inputs: bfloat16 [131072, 2048], P('fs'), may hold values from -6 to 6
- unit_cotangent: bfloat16 [131072, 2560], P('fs', 'tp'), may hold values from -0.049560547 to 0.049560547
- gated_states: bfloat16 [131072, 2560], P('fs', 'tp'), may hold values from -6 to 6
- mixer_cotangent: bfloat16 [131072, 2048], P('fs'), may hold values from -0.049560547 to 0.049560547
- left_factor: bfloat16 [2048, 256], replicated, may hold values from -0.125 to 0.125
- right_factor: bfloat16 [2048, 256], replicated, may hold values from -0.125 to 0.125
- master_input: float32 [2048, 2560], P('fs', 'tp'), may hold values from -6 to 6
- master_output: float32 [2560, 2048], P('tp', 'fs'), may hold values from -6 to 6
- moment_input: float32 [256, 2560], P('fs', 'tp'), may hold values from -80 to 80
- moment_output: float32 [256, 2560], P('fs', 'tp'), may hold values from -80 to 80
- square_input: float32 [256, 2560], P('fs', 'tp'), may hold values from 0.1 to 4
- square_output: float32 [256, 2560], P('fs', 'tp'), may hold values from 0.1 to 4
Outputs:
- first_input: float32 [256, 2560], P('fs', 'tp')
- first_output: float32 [256, 2560], P('fs', 'tp')
- second_input: float32 [256, 2560], P('fs', 'tp')
- second_output: float32 [256, 2560], P('fs', 'tp')
- step_input: float32 [2048, 2560], P('fs', 'tp')
- step_output: float32 [2560, 2048], P('tp', 'fs')
- weight_input: float32 [2048, 2560], P('fs', 'tp')
- weight_output: float32 [2560, 2048], P('tp', 'fs')
- copy_input: bfloat16 [2048, 2560], P('fs', 'tp')
- copy_output: bfloat16 [2560, 2048], P('tp', 'fs')
All inputs are finite; a program needn't handle non-finite values.
Results may differ from a plain program's by a relative error of at most 0.002.
Values sent between devices are 32-bit elements; how exact they have to be, the bound alone decides.
A program may use at most 32 MiB of HBM per device.

v0:
```python
import functools

import jax
import jax.numpy as jnp
from jax import lax
from jax.sharding import Mesh
from jax.sharding import PartitionSpec as P

FS = ("fs_0", "fs_1", "fs_2")
FS_TP = ("fs_0", "fs_1", "fs_2", "tp")


first_decay = 0.9
second_decay = 0.95
divide_guard = 1e-08
mean_guard = 1e-06
clip_level = 0.1


def own_block(pieces, axes, sequence):
    inside = pieces.shape[1:]
    pieces = pieces.reshape(*(lax.axis_size(a) for a in axes), *inside)
    pieces = jnp.moveaxis(pieces, sequence, range(len(axes))).reshape(-1, *inside)
    for k in sequence:
        pieces = lax.psum_scatter(pieces, axes[k], scatter_dimension=0, tiled=True)
    return pieces[0]


def split_up(array, dim, length):
    before, after = (array.shape[:dim], array.shape[dim + 1 :])
    return jnp.moveaxis(array.reshape(*before, length, -1, *after), dim, 0)


def sum_by_axis(array, axes, sequence, dim):
    length = lax.axis_size(axes)
    return own_block(split_up(array, dim, length), axes, sequence)


def by_axis(array, axes):
    return functools.reduce(lax.psum, axes, array)


def laid_out(pieces, dim):
    lengths = list(pieces.shape[1:])
    lengths[dim] *= pieces.shape[0]
    return jnp.moveaxis(pieces, 0, dim).reshape(lengths)


def all_blocks(array, axes, sequence):
    pieces = array[None]
    for k in sequence:
        pieces = lax.all_gather(pieces, axes[k], axis=0, tiled=True)
    current = [lax.axis_size(axes[k]) for k in reversed(sequence)]
    pieces = pieces.reshape(*current, *array.shape)
    turned = sorted(range(len(sequence)), key=lambda place: sequence[len(sequence) - 1 - place])
    return pieces.transpose(*turned, *range(len(sequence), pieces.ndim)).reshape(-1, *array.shape)


def whole_of(array, axes, sequence, dim):
    return laid_out(all_blocks(array, axes, sequence), dim)


def contract_tokens(left, right):
    return lax.dot_general(
        left, right, (((0,), (0,)), ((), ())), preferred_element_type=jnp.float32
    )


def moment_update(moment, square, projected):
    first = first_decay * moment + (1.0 - first_decay) * projected
    second = second_decay * square + (1.0 - second_decay) * projected * projected
    heading = first / (jnp.sqrt(second) + divide_guard)
    return (first, second, heading)


def shards(
    saved_inputs,
    unit_cotangent,
    gated_states,
    mixer_cotangent,
    left_factor,
    right_factor,
    master_input,
    master_output,
    moment_input,
    moment_output,
    square_input,
    square_output,
):
    in_rows = jnp.dot(saved_inputs, left_factor, preferred_element_type=jnp.float32).astype(
        jnp.bfloat16
    )
    out_rows = jnp.dot(mixer_cotangent, right_factor, preferred_element_type=jnp.float32).astype(
        jnp.bfloat16
    )
    shard_rows = moment_input.shape[0]
    width = unit_cotangent.shape[1]
    joint = sum_by_axis(
        jnp.concatenate(
            [contract_tokens(in_rows, unit_cotangent), contract_tokens(out_rows, gated_states)],
            axis=1,
        ),
        FS,
        (2, 1, 0),
        0,
    )
    proj_in = joint[:, :width]
    proj_out = joint[:, width:]
    first_input, second_input, heading_input = moment_update(moment_input, square_input, proj_in)
    first_output, second_output, heading_output = moment_update(
        moment_output, square_output, proj_out
    )
    totals = (
        by_axis(jnp.sum(heading_input * heading_input), FS_TP),
        by_axis(jnp.sum(heading_output * heading_output), FS_TP),
    )
    local_width = master_input.shape[0]
    offset = lax.axis_index(FS) * local_width
    left_local = lax.dynamic_slice_in_dim(left_factor, offset, local_width, 0).astype(jnp.float32)
    right_local = lax.dynamic_slice_in_dim(right_factor, offset, local_width, 0).astype(jnp.float32)
    columns = left_local
    block_input = jnp.dot(
        columns, whole_of(heading_input, FS, (0, 1, 2), 0), precision=lax.Precision.HIGHEST
    )
    columns = right_local
    block_output = lax.dot_general(
        whole_of(heading_output, FS, (0, 1, 2), 0),
        columns,
        (((0,), (1,)), ((), ())),
        precision=lax.Precision.HIGHEST,
    )
    entries = shard_rows * lax.axis_size(FS) * width * lax.axis_size("tp")
    gain_input = jnp.minimum(1.0, clip_level / jnp.sqrt(totals[0] / entries + mean_guard))
    gain_output = jnp.minimum(1.0, clip_level / jnp.sqrt(totals[1] / entries + mean_guard))
    step_input = gain_input * block_input
    step_output = gain_output * block_output
    weight_input = master_input - step_input
    weight_output = master_output - step_output
    return (
        first_input,
        first_output,
        second_input,
        second_output,
        step_input,
        step_output,
        weight_input,
        weight_output,
        weight_input.astype(jnp.bfloat16),
        weight_output.astype(jnp.bfloat16),
    )


def solution(mesh):
    finer = Mesh(mesh.devices.reshape(32, 4, 2, mesh.shape["tp"]), ("fs_0", "fs_1", "fs_2", "tp"))
    in_specs = (
        P(FS, None),
        P(FS, "tp"),
        P(FS, "tp"),
        P(FS, None),
        P(),
        P(),
        P(FS, "tp"),
        P("tp", FS),
        P(FS, "tp"),
        P(FS, "tp"),
        P(FS, "tp"),
        P(FS, "tp"),
    )
    out_specs = (
        P(FS, "tp"),
        P(FS, "tp"),
        P(FS, "tp"),
        P(FS, "tp"),
        P(FS, "tp"),
        P("tp", FS),
        P(FS, "tp"),
        P("tp", FS),
        P(FS, "tp"),
        P("tp", FS),
    )
    return jax.shard_map(
        shards, mesh=finer, in_specs=in_specs, out_specs=out_specs, check_vma=False
    )
```

profile of v0, /device:TPU:1, one launch (start us, length us, event | category | flops | bytes accessed | tf_op | source)
XLA Modules:
  0.0 605.1 jit_solution(940509205364172843)
XLA Ops:
  7.2 0.0 copy-start
  7.2 0.0 copy-start.7
  7.2 0.0 reduce-scatter.4.cloned.1.call-start
  7.2 1.5 copy-done
  8.8 3.6 fusion
  12.4 0.0 copy-done.7
  12.4 3.9 fusion.1
  16.4 1.4 pad_maximum_fusion
  17.7 1.9 reshape_reshape.9
  19.6 0.0 copy-start.3
  19.6 0.0 copy-start.4
  19.6 0.0 copy-start.5
  19.6 0.0 copy-start.6
  19.6 2.9 copy.26
  22.5 0.0 reduce-scatter.4.cloned.1.call-update
  22.5 0.0 reduce-scatter.6.cloned.1.call-start
  22.5 40.6 %reduce-scatter.4.cloned.1.call-done = f32[128,1,1280]{2,0,1:T(8,128)} async-done(((f32[256,1,1280]{2,0,1:T(8,128)}), f32[128,1,1280]{2,0,1:T(8,128)}) %reduce-scatter.4.cloned.1.call-update) | async-done | bytes 655376 | tf_op jit(solution)/shard_map/reduce_scatter | solution.py:25
  63.2 0.0 reduce-scatter.6.cloned.1.call-update
  63.2 0.0 all-reduce.7.cloned.1.call-start
  63.2 40.3 %reduce-scatter.6.cloned.1.call-done = f32[32,1,1280]{2,0,1:T(8,128)} async-done(((f32[128,1,1280]{2,0,1:T(8,128)}), f32[32,1,1280]{2,0,1:T(8,128)}) %reduce-scatter.6.cloned.1.call-update) | async-done | bytes 163856 | tf_op jit(solution)/shard_map/reduce_scatter | solution.py:25
  103.5 0.0 all-reduce.7.cloned.1.call-update
  103.6 1.3 dynamic-slice
  104.8 246.0 %all-reduce.7.cloned.1.call-done = f32[32,1,1280]{2,0,1:T(8,128)} async-done(((f32[32,1,1280]{2,0,1:T(8,128)}), f32[32,1,1280]{2,0,1:T(8,128)}) %all-reduce.7.cloned.1.call-update) | async-done | bytes 163856
  350.8 1.4 dynamic-slice_bitcast_fusion
  352.2 0.0 copy-done.3
  352.2 0.0 copy-done.4
  352.3 0.0 copy-done.5
  352.3 0.0 copy-done.6
  352.3 1.2 multiply_reduce_fusion
  353.5 42.0 %all-reduce.1 = (f32[]{:T(128)}, f32[]{:T(128)}) all-reduce(f32[]{:T(128)} %get-tuple-element.30, f32[]{:T(128)} %get-tuple-element.22), channel_id=1, replica_groups=mesh['fs_0'=32,'fs_1'=4,'fs_2'=2,'tp'=4] {'fs_0'}, use_global_device_ids=true, to_apply=%region_4.0 | all-reduce | flops 2 | bytes 16 | tf_op jit(solution)/shard_map/psum | solution.py:40
  395.5 9.0 %all-reduce.3 = (f32[]{:T(128)}, f32[]{:T(128)}) all-reduce(f32[]{:T(128)} %get-tuple-element.10, f32[]{:T(128)} %get-tuple-element.11), channel_id=1, replica_groups=mesh['fs_0'=32,'fs_1'=4,'fs_2'=2,'tp'=4] {'fs_1'}, use_global_device_ids=true, to_apply=%region_5.0 | all-reduce | flops 2 | bytes 16 | tf_op jit(solution)/shard_map/psum | solution.py:40
  404.5 39.8 %all-reduce.4 = (f32[]{:T(128)}, f32[]{:T(128)}) all-reduce(f32[]{:T(128)} %get-tuple-element.14, f32[]{:T(128)} %get-tuple-element.15), channel_id=1, replica_groups=mesh['fs_0'=32,'fs_1'=4,'fs_2'=2,'tp'=4] {'fs_2'}, use_global_device_ids=true, to_apply=%region_6.0 | all-reduce | flops 2 | bytes 16 | tf_op jit(solution)/shard_map/psum | solution.py:40
  444.3 9.1 %all-reduce.2 = (f32[]{:T(128)}, f32[]{:T(128)}) all-reduce(f32[]{:T(128)} %get-tuple-element.16, f32[]{:T(128)} %get-tuple-element.17), channel_id=1, replica_groups=mesh['fs_0'=32,'fs_1'=4,'fs_2'=2,'tp'=4] {'tp'}, use_global_device_ids=true, to_apply=%region_7.0 | all-reduce | flops 2 | bytes 16 | tf_op jit(solution)/shard_map/psum | solution.py:40
  454.0 39.3 %all-gather.7 = f32[32,1,640]{2,1,0:T(1,128)S(1)} all-gather(f32[1,1,640]{2,1,0:T(1,128)S(1)} %bitcast.38), channel_id=5, replica_groups=mesh['fs_0'=32,'fs_1'=4,'fs_2'=2,'tp'=4] {'fs_0'}, dimensions={0}, use_global_device_ids=true | all-gather | bytes 84480 | tf_op jit(solution)/shard_map/all_gather | solution.py:52
  493.3 9.5 %all-gather.4 = f32[128,640]{1,0:T(8,128)S(1)} all-gather(f32[32,640]{1,0:T(8,128)S(1)} %bitcast.35), channel_id=6, replica_groups=mesh['fs_0'=32,'fs_1'=4,'fs_2'=2,'tp'=4] {'fs_1'}, dimensions={0}, use_global_device_ids=true | all-gather | bytes 409600 | tf_op jit(solution)/shard_map/all_gather | solution.py:52
  502.8 20.8 %all-gather.5 = f32[256,640]{1,0:T(8,128)S(1)} all-gather(f32[128,640]{1,0:T(8,128)S(1)} %all-gather.4), channel_id=7, replica_groups=mesh['fs_0'=32,'fs_1'=4,'fs_2'=2,'tp'=4] {'fs_2'}, dimensions={0}, use_global_device_ids=true | all-gather | bytes 983040 | tf_op jit(solution)/shard_map/all_gather | solution.py:52
  523.6 0.5 copy.28
  524.1 0.5 reshape_reshape.11
  525.3 38.0 %all-gather.6 = f32[32,1,640]{2,1,0:T(1,128)S(1)} all-gather(f32[1,1,640]{2,1,0:T(1,128)S(1)} %bitcast.37), channel_id=2, replica_groups=mesh['fs_0'=32,'fs_1'=4,'fs_2'=2,'tp'=4] {'fs_0'}, dimensions={0}, use_global_device_ids=true | all-gather | bytes 84480 | tf_op jit(solution)/shard_map/all_gather | solution.py:52
  563.3 0.0 copy-start.1
  563.4 9.5 %all-gather.1 = f32[128,640]{1,0:T(8,128)S(1)} all-gather(f32[32,640]{1,0:T(8,128)S(1)} %bitcast.36), channel_id=3, replica_groups=mesh['fs_0'=32,'fs_1'=4,'fs_2'=2,'tp'=4] {'fs_1'}, dimensions={0}, use_global_device_ids=true | all-gather | bytes 409600 | tf_op jit(solution)/shard_map/all_gather | solution.py:52
  572.9 19.5 %all-gather.2 = f32[256,640]{1,0:T(8,128)S(1)} all-gather(f32[128,640]{1,0:T(8,128)S(1)} %all-gather.1), channel_id=4, replica_groups=mesh['fs_0'=32,'fs_1'=4,'fs_2'=2,'tp'=4] {'fs_2'}, dimensions={0}, use_global_device_ids=true | all-gather | bytes 983040 | tf_op jit(solution)/shard_map/all_gather | solution.py:52
  592.3 1.3 copy.27
  593.7 1.5 reshape_reshape.10
  595.2 0.0 copy-done.1
  595.2 1.6 fusion.8
  596.9 0.0 copy-done.2
  596.9 1.6 fusion.9
  (3 shorter events, 0.0 us)
Async XLA Ops:
  7.2 1.6 copy-start
  7.2 5.2 copy-start.7
  7.2 56.0 %reduce-scatter.4.cloned.1.call-start = ((), (), s32[]{:S(2)}) async-start(), calls=%async_computation.2 | async-start | bytes 1966080 | tf_op jit(solution)/shard_map/reduce_scatter | solution.py:25
  19.6 332.6 %copy-start.3 = (f32[1,640]{1,0:T(1,128)S(1)}, f32[1,640]{1,0:T(1,128)}, u32[]{:S(2)}) copy-start(f32[1,640]{1,0:T(1,128)} %param.23) | copy-start | bytes 7684
  19.6 332.6 %copy-start.4 = (f32[1,640]{1,0:T(1,128)S(1)}, f32[1,640]{1,0:T(1,128)}, u32[]{:S(2)}) copy-start(f32[1,640]{1,0:T(1,128)} %param.21) | copy-start | bytes 7684
  19.6 332.7 %copy-start.5 = (f32[1,640]{1,0:T(1,128)S(1)}, f32[1,640]{1,0:T(1,128)}, u32[]{:S(2)}) copy-start(f32[1,640]{1,0:T(1,128)} %param.22) | copy-start | bytes 7684
  19.6 332.7 %copy-start.6 = (f32[1,640]{1,0:T(1,128)S(1)}, f32[1,640]{1,0:T(1,128)}, u32[]{:S(2)}) copy-start(f32[1,640]{1,0:T(1,128)} %param.20) | copy-start | bytes 7684
  22.5 81.0 %reduce-scatter.6.cloned.1.call-start = ((), (), s32[]{:S(2)}) async-start(), calls=%async_computation.3 | async-start | bytes 819200 | tf_op jit(solution)/shard_map/reduce_scatter | solution.py:25
  63.2 287.6 %all-reduce.7.cloned.1.call-start = ((), (), s32[]{:S(2)}) async-start(), calls=%async_computation.4 | async-start | bytes 327680
  563.3 31.9 %copy-start.1 = (f32[640,8]{0,1:T(8,128)S(1)}, f32[640,8]{0,1:T(8,128)}, u32[]{:S(2)}) copy-start(f32[640,8]{0,1:T(8,128)} %param.19) | copy-start | bytes 61444
  572.9 24.0 %copy-start.2 = (f32[8,640]{1,0:T(8,128)S(1)}, f32[8,640]{1,0:T(8,128)}, u32[]{:S(2)}) copy-start(f32[8,640]{1,0:T(8,128)} %param.18) | copy-start | bytes 61444
Sparse Core Ops, SparseCore 0:
  22.6 40.5 reduce-scatter.3
  66.6 36.9 reduce-scatter.5
  105.9 244.9 all-reduce.6
where the time goes:
time: 606 us; the launch traced here: 605 us
  waiting for transfers between devices  327 us (54%)
  blocking collectives  236 us (39%)
  between operations  15.2 us (3%)
  local copies, waits for them, and re-layouts  12.8 us (2%)
  matrix products  10.9 us (2%)
    unnamed x4, waiting for transfers between devices  246 us
    all_gather x6, blocking collectives, all_blocks(): pieces = lax.all_gather(pieces, axes[k], axis=0, tiled=True)  137 us
    psum x4, blocking collectives, by_axis(): return functools.reduce(lax.psum, axes, array)  99.9 us
    reduce_scatter x2, waiting for transfers between devices, own_block(): pieces = lax.psum_scatter(pieces, axes[k], scatter_dimension=0, tiled=True)  80.9 us
  transfers between devices with their start and end apart: 3, of which 3 were waited for; matrix products, arithmetic and copies ran while one was open for 0% of the time, Pallas kernels for 0%

commit v1 on v0

v1 whole, which is shorter than its diff:
```python
import functools

import jax
import jax.numpy as jnp
from jax import lax
from jax.experimental import pallas as pl
from jax.experimental.pallas import tpu as pltpu
from jax.sharding import Mesh
from jax.sharding import PartitionSpec as P

FS = ("fs_0", "fs_1", "fs_2")
MESH = pl.DeviceIdType.MESH

first_decay = 0.9
second_decay = 0.95
divide_guard = 1e-08
mean_guard = 1e-06
clip_level = 0.1


def near(x):
    return x + 1 - 2 * lax.rem(x, 2)


def permutation(nz, nx):
    n = 2 * nz * nx
    p = lax.broadcasted_iota(jnp.int32, (n, n), 0)
    r = lax.broadcasted_iota(jnp.int32, (n, n), 1)
    bits_z = (2 * nz).bit_length() - 1
    bits_x = (2 * nx).bit_length() - 1
    px = lax.shift_right_logical(p, bits_z)
    rest = lax.bitwise_and(p, 2 * nz - 1)
    pz = lax.shift_right_logical(rest, 1)
    pc = lax.bitwise_and(rest, 1)
    want = lax.shift_left(pz, bits_x) + 2 * px + pc
    return jnp.where(want == r, 1.0, 0.0).astype(jnp.bfloat16)


def dot_t(a, b):
    return lax.dot_general(a, b, (((1,), (1,)), ((), ())), preferred_element_type=jnp.float32)


def exchange(
    nz, nx, ny, entries,
    a0, u0, u1, a1, l0, l1, m0, m1, s0, s1,
    out_step, out_fs,
    X, F, U, PS, CR, S, XA, XB, FA, FB, XA2, XB2, T, ZS, ZR, ZG, HX, MS, MR, FO, Q, QY, QX, ST,
    load_sem, core_send, core_recv, x_send, x_recv, z_send, z_recv, q_send, q_recv,
):
    z = lax.axis_index("fs_0")
    x = lax.axis_index("fs_1")
    c = lax.axis_index("fs_2")
    y = lax.axis_index("tp")
    other = 1 - c
    xa = near(x)
    xb = nx - 1 - x
    xo = lax.rem(x + 2, nx)
    nh = nz
    W = u0.shape[1]

    def z_offset(i):
        step = lax.div(i, 2)
        return lax.rem(z + nz + (nz // 2 - step) * (1 - 2 * lax.rem(i, 2)) + nz, nz)

    barrier = pltpu.get_barrier_semaphore()

    def greet(i, carry):
        pl.semaphore_signal(barrier, inc=1, device_id={"fs_0": z_offset(i)}, device_id_type=MESH)
        return carry

    lax.fori_loop(0, nz - 1, lambda i, t: greet(jnp.where(i == 0, 0, i + 1), t), 0)
    pl.semaphore_signal(barrier, inc=1, device_id={"fs_2": other}, device_id_type=MESH)
    for d in range(1, nx):
        pl.semaphore_signal(barrier, inc=1, device_id={"fs_1": lax.rem(x + d, nx)}, device_id_type=MESH)
    for d in range(1, ny):
        pl.semaphore_signal(barrier, inc=1, device_id={"tp": lax.rem(y + d, ny)}, device_id_type=MESH)

    loads = []
    for k, (src, dst) in enumerate((
        (l0, F.at[0]), (a0, X.at[0]), (u0, U.at[0]),
        (l1, F.at[1]), (a1, X.at[1]), (u1, U.at[1]),
        (m0, MS.at[0, 0]), (s0, MS.at[0, 1]), (m1, MS.at[1, 0]), (s1, MS.at[1, 1]),
    )):
        cp = pltpu.make_async_copy(src, dst, load_sem.at[k])
        cp.start()
        loads.append(cp)
    perm = permutation(nz, nx)
    for cp in loads:
        cp.wait()

    def project(k, carry):
        m = lax.rem(other + k, 2)
        rows = jnp.dot(X[m], F[m], preferred_element_type=jnp.float32).astype(jnp.bfloat16)
        turned = dot_t(perm, rows).astype(jnp.bfloat16)
        PS[m] = jnp.dot(turned, U[m], preferred_element_type=jnp.float32)
        return carry

    lax.fori_loop(0, 2, project, 0)

    pl.semaphore_wait(barrier, 1 + (nx - 1) + (ny - 1) + (nz - 1))

    def remote(src, dst, send, recv, **where):
        return pltpu.make_async_remote_copy(
            src_ref=src, dst_ref=dst, send_sem=send, recv_sem=recv, device_id=where, device_id_type=MESH
        )

    give = remote(PS.at[other], CR, core_send.at[0], core_recv.at[0], fs_2=other)
    give.start()
    give_m = remote(MS.at[other], MR, core_send.at[1], core_recv.at[1], fs_2=other)
    give_m.start()
    give.wait_recv()
    S[...] = (PS[c] + CR[...]).reshape(nx, 2 * nz, W)

    lo, hi = pl.ds(0, nh), pl.ds(nh, nh)
    c_a1 = remote(S.at[xo, lo], XA.at[1], x_send.at[0], x_recv.at[0], fs_1=xa)
    c_b1 = remote(S.at[xo, hi], XB.at[1], x_send.at[1], x_recv.at[1], fs_1=xb)
    c_a0 = remote(S.at[xa, lo], XA.at[0], x_send.at[2], x_recv.at[2], fs_1=xa)
    c_b0 = remote(S.at[xb, hi], XB.at[0], x_send.at[3], x_recv.at[3], fs_1=xb)
    for cp in (c_a1, c_b1, c_a0, c_b0):
        cp.start()
    c_a1.wait_recv()
    FA[...] = S[xb, 0:nh] + XA[1]
    c_fa = remote(FA, XA2, x_send.at[4], x_recv.at[4], fs_1=xb)
    c_fa.start()
    c_b1.wait_recv()
    FB[...] = S[xa, nh : 2 * nh] + XB[1]
    c_fb = remote(FB, XB2, x_send.at[5], x_recv.at[5], fs_1=xa)
    c_fb.start()
    c_a0.wait_recv()
    T[0:nh] = S[x, 0:nh] + XA[0]
    c_b0.wait_recv()
    T[nh : 2 * nh] = S[x, nh : 2 * nh] + XB[0]
    c_fa.wait_recv()
    T[0:nh] = T[0:nh] + XA2[...]
    c_fb.wait_recv()
    T[nh : 2 * nh] = T[nh : 2 * nh] + XB2[...]
    for j in range(nz):
        ZS[j] = T[2 * j : 2 * j + 2]

    def scatter(i, carry):
        t = z_offset(jnp.where(i == 0, 0, i + 1))
        remote(ZS.at[t], ZR.at[i], z_send.at[0], z_recv.at[0], fs_0=t).start()
        return carry

    lax.fori_loop(0, nz - 1, scatter, 0)
    all_in = remote(ZR, ZR, z_send.at[0], z_recv.at[0], fs_0=lax.rem(z + 1, nz))
    all_in.wait_recv()
    proj = ZS[z] + jnp.sum(ZR[...], axis=0)

    give_m.wait_recv()

    def both(own, got):
        top = jnp.where(c == 0, own, got)
        low = jnp.where(c == 0, got, own)
        return jnp.concatenate([top, low], axis=0)

    moment = both(MS[c, 0], MR[0])
    square = both(MS[c, 1], MR[1])
    first = first_decay * moment + (1.0 - first_decay) * proj
    second = second_decay * square + (1.0 - second_decay) * proj * proj
    heading = first / (jnp.sqrt(second) + divide_guard)
    ZG[z] = heading

    def spread(i, carry):
        t = z_offset(jnp.where(i == 0, 0, i + 1))
        remote(ZG.at[z], ZG.at[z], z_send.at[1], z_recv.at[1], fs_0=t).start()
        return carry

    lax.fori_loop(0, nz - 1, spread, 0)

    out_fs[c, 0] = jnp.where(c == 0, first[0:1], first[1:2])
    out_fs[c, 1] = jnp.where(c == 0, second[0:1], second[1:2])
    FO[0] = jnp.where(c == 0, first[1:2], first[0:1])
    FO[1] = jnp.where(c == 0, second[1:2], second[0:1])
    give_f = remote(FO, out_fs.at[c], core_send.at[2], core_recv.at[2], fs_2=other)
    give_f.start()

    start = pl.multiple_of((z * nx + x) * 16, 16)
    factor = dot_t(F[c, pl.ds(start, 16), :], perm)

    all_out = remote(ZR, ZR, z_send.at[1], z_recv.at[1], fs_0=lax.rem(z + 1, nz))
    all_out.wait_recv()
    for j in range(nz):
        HX[x, 2 * j : 2 * j + 2] = ZG[j]

    g = [
        remote(HX.at[x, lo], HX.at[x, lo], x_send.at[6], x_recv.at[6], fs_1=xb),
        remote(HX.at[x, hi], HX.at[x, hi], x_send.at[7], x_recv.at[7], fs_1=xa),
        remote(HX.at[x, lo], HX.at[x, lo], x_send.at[8], x_recv.at[8], fs_1=xa),
        remote(HX.at[x, hi], HX.at[x, hi], x_send.at[9], x_recv.at[9], fs_1=xb),
    ]
    for cp in g:
        cp.start()

    mine = HX[x]
    squares = jnp.sum((mine * mine).reshape(2 * nz // 8, 8, W), axis=0)
    total = squares[:, 0:128]
    for k in range(1, W // 128):
        total = total + squares[:, k * 128 : (k + 1) * 128]
    Q[0] = total
    if ny > 1:
        for d in range(1, ny):
            remote(Q.at[0], QY.at[d - 1], q_send.at[0], q_recv.at[0], tp=lax.rem(y + d, ny)).start()

    g[0].wait_recv()
    f0 = remote(HX.at[xb, lo], HX.at[xb, lo], x_send.at[10], x_recv.at[10], fs_1=xa)
    f0.start()
    g[1].wait_recv()
    f1 = remote(HX.at[xa, hi], HX.at[xa, hi], x_send.at[11], x_recv.at[11], fs_1=xb)
    f1.start()

    if ny > 1:
        y_all = remote(QY, QY, q_send.at[0], q_recv.at[0], tp=lax.rem(y + 1, ny))
        y_all.wait_recv()
        total = total + jnp.sum(QY[...], axis=0)
    Q[1] = total
    for d in range(1, nx):
        remote(Q.at[1], QX.at[d - 1], q_send.at[1], q_recv.at[1], fs_1=lax.rem(x + d, nx)).start()
    x_all = remote(QX, QX, q_send.at[1], q_recv.at[1], fs_1=lax.rem(x + 1, nx))
    x_all.wait_recv()
    total = total + jnp.sum(QX[...], axis=0)
    mean = jnp.sum(jnp.sum(total, axis=1, keepdims=True), axis=0, keepdims=True) / entries
    gain = jnp.minimum(1.0, clip_level / jnp.sqrt(mean + mean_guard))

    for cp in (g[2], g[3], f0, f1):
        cp.wait_recv()
    block = jnp.dot(
        factor, HX[...].reshape(2 * nz * nx, W),
        precision=lax.Precision.HIGHEST, preferred_element_type=jnp.float32,
    )
    step = gain * block
    ST[...] = step.reshape(2, 8, W)
    give_s = remote(ST.at[other], out_step.at[c], core_send.at[3], core_recv.at[3], fs_2=other)
    give_s.start()
    out_step[c] = ST[c]

    give.wait_send()
    give_m.wait_send()
    for cp in (c_a1, c_b1, c_a0, c_b0, c_fa, c_fb, *g, f0, f1):
        cp.wait_send()
    all_in.wait_send()
    all_out.wait_send()
    if ny > 1:
        y_all.wait_send()
    x_all.wait_send()
    give_f.wait()
    give_s.wait()


def finish(step, fs, mi, mo, fi, fo, si, so, ti, to, wi, wo, ci, co):
    fi[...] = fs[0, 0]
    si[...] = fs[0, 1]
    fo[...] = fs[1, 0]
    so[...] = fs[1, 1]
    s = step[0]
    ti[...] = s
    w = mi[...] - s
    wi[...] = w
    ci[...] = w.astype(jnp.bfloat16)
    s = step[1]
    to[...] = s
    w = mo[...] - s
    wo[...] = w
    co[...] = w.astype(jnp.bfloat16)


def shards(nz, nx, ny, saved, unit, gated, mixer, left, right, mi, mo, m0, m1, s0, s1):
    f32, bf16 = jnp.float32, jnp.bfloat16
    n, d = saved.shape
    W = unit.shape[1]
    rank = left.shape[1]
    assert rank == 2 * nz * nx and nx == 4 and mi.shape[0] == 8 and m0.shape[0] == 1
    entries = float(rank * W * ny)
    V = pltpu.VMEM
    dma = pltpu.SemaphoreType.DMA
    half = nz
    anywhere = pl.BlockSpec(memory_space=pl.ANY)
    vmem = pl.BlockSpec(memory_space=pltpu.VMEM)
    step, fs = pl.pallas_call(
        functools.partial(exchange, nz, nx, ny, entries),
        out_shape=(
            jax.ShapeDtypeStruct((2, 8, W), f32),
            jax.ShapeDtypeStruct((2, 2, 1, W), f32),
        ),
        in_specs=[anywhere] * 10,
        out_specs=(vmem, vmem),
        scratch_shapes=[
            V((2, n, d), bf16),
            V((2, d, rank), bf16),
            V((2, n, W), bf16),
            V((2, rank, W), f32),
            V((rank, W), f32),
            V((nx, 2 * nz, W), f32),
            V((2, half, W), f32),
            V((2, half, W), f32),
            V((half, W), f32),
            V((half, W), f32),
            V((half, W), f32),
            V((half, W), f32),
            V((2 * nz, W), f32),
            V((nz, 2, W), f32),
            V((nz - 1, 2, W), f32),
            V((nz, 2, W), f32),
            V((nx, 2 * nz, W), f32),
            V((2, 2, 1, W), f32),
            V((2, 1, W), f32),
            V((2, 1, W), f32),
            V((2, 8, 128), f32),
            V((max(ny - 1, 1), 8, 128), f32),
            V((nx - 1, 8, 128), f32),
            V((2, 8, W), f32),
            dma((10,)),
            dma((4,)),
            dma((4,)),
            dma((12,)),
            dma((12,)),
            dma((2,)),
            dma((2,)),
            dma((2,)),
            dma((2,)),
        ],
        compiler_params=pltpu.CompilerParams(collective_id=0, has_side_effects=True),
        name="exchange",
    )(saved, unit, gated, mixer, left, right, m0, m1, s0, s1)
    row = jax.ShapeDtypeStruct((1, W), f32)
    outs = pl.pallas_call(
        finish,
        out_shape=(
            row, row, row, row,
            jax.ShapeDtypeStruct((8, W), f32),
            jax.ShapeDtypeStruct((8, W), f32),
            jax.ShapeDtypeStruct((8, W), f32),
            jax.ShapeDtypeStruct((8, W), f32),
            jax.ShapeDtypeStruct((8, W), bf16),
            jax.ShapeDtypeStruct((8, W), bf16),
        ),
        name="finish",
    )(step, fs, mi, mo.T)
    return tuple(out.T if k in (5, 7, 9) else out for k, out in enumerate(outs))


def solution(mesh):
    ny = mesh.shape["tp"]
    nx = 4
    nz = mesh.shape["fs"] // (2 * nx)
    finer = Mesh(mesh.devices.reshape(nz, nx, 2, ny), (*FS, "tp"))
    rows, cols = P(FS, "tp"), P("tp", FS)
    return jax.shard_map(
        functools.partial(shards, nz, nx, ny),
        mesh=finer,
        in_specs=(P(FS, None), rows, rows, P(FS, None), P(), P(), rows, cols, rows, rows, rows, rows),
        out_specs=(rows, rows, rows, rows, rows, cols, rows, cols, rows, cols),
        check_vma=False,
    )
```

time: 606 us -> 88.3 us (0.15)
  waiting for transfers between devices: 327 us -> 0 us
  blocking collectives: 236 us -> 0 us
  Pallas kernels: 0 us -> 87.5 us
  between operations: 15.2 us -> 0.65 us
  local copies, waits for them, and re-layouts: 12.8 us -> 0 us
  matrix products: 10.9 us -> 0 us
    unnamed x4 -> x0, waiting for transfers between devices: 246 us -> none
    all_gather x6 -> x0, blocking collectives: 137 us -> none  [all_blocks(): pieces = lax.all_gather(pieces, axes[k], axis=0, tiled=True)]
    psum x4 -> x0, blocking collectives: 99.9 us -> none  [by_axis(): return functools.reduce(lax.psum, axes, array)]
    pallas_call x0 -> x2, Pallas kernels: none -> 87.5 us  [the longest x1 86 us: shards(): pl.pallas_call(functools.partial(exchange, nz, nx, ny, entries), out_shap...]
    reduce_scatter x2 -> x0, waiting for transfers between devices: 80.9 us -> none  [own_block(): pieces = lax.psum_scatter(pieces, axes[k], scatter_dimension=0, tiled=True)]
    dot_general x4 -> x0, matrix products: 10.9 us -> none  [the longest x2 7.59 us: contract_tokens(): lax.dot_general(left, right, (((0,), (0,)), ((), ())), preferred_element_...]
    another operation x4 -> x0, local copies, waits for them, and re-layouts: 6.7 us -> none  [the longest x2 4.71 us: own_block(): pieces = pieces.reshape(*(lax.axis_size(a) for a in axes), *inside)]
  transfers between devices with their start and end apart: 3 -> 0, of which waited for: 3 -> 0; matrix products, arithmetic and copies ran while one was open for 0% -> 0% of each run, Pallas kernels for 0% -> 0%
where the time goes in v1:
time: 88.3 us; the launch traced here: 88.1 us
  Pallas kernels  87.5 us (99%)
    pallas_call x1, Pallas kernels, shards(): pl.pallas_call(functools.partial(exchange, nz, nx, ny, entries), out_shap...  86 us

profile of v1, /device:TPU:1, one launch (start us, length us, event | category | flops | bytes accessed | tf_op | source)
XLA Modules:
  0.0 88.1 jit_solution(513445269502566437)
XLA Ops:
  0.6 86.0 %exchange.1 = (f32[2,8,640]{2,1,0:T(8,128)}, f32[2,2,1,640]{3,2,1,0:T(1,128)}) custom-call(bf16[512,2048]{1,0:T(8,128)(2,1)} %a0.1, bf16[512,640]{1,0:T(8,128)(2,1)} %u0.1, bf16[512,640]{1,0:T(8,128)(2,1)} %u1_.1, bf16[512,2048]{1,0:T(8,128)(2,1)} %a1.1, bf16[2048,256]{1,0:T(8,128)(2,1)} %l0.1, bf16[2048,256]{1,0:T(8,128)(2,1)} %l1.1, f32[1,640]{1,0:T(1,128)} %m0.1, ...), custom_call_target="tpu_custom_call" | custom-call | tf_op jit(solution)/shard_map/exchange/pallas_call | solution.py:279
  86.7 1.5 %finish.1 = (f32[1,640]{1,0:T(1,128)}, f32[1,640]{1,0:T(1,128)}, f32[1,640]{1,0:T(1,128)}, f32[1,640]{1,0:T(1,128)}, f32[8,640]{1,0:T(8,128)}, /*index=5*/f32[8,...) custom-call(f32[2,8,640]{2,1,0:T(8,128)} %get-tuple-element.22.step, ...), custom_call_target="tpu_custom_call" | custom-call | tf_op jit(solution)/shard_map/finish/pallas_call | solution.py:326

commit v2 on v0

v2 whole, which is shorter than its diff:
```python
import functools

import jax
import jax.numpy as jnp
from jax import lax
from jax.experimental import pallas as pl
from jax.experimental.pallas import tpu as pltpu
from jax.sharding import Mesh
from jax.sharding import PartitionSpec as P

FS = ("fs_0", "fs_1", "fs_2")
MESH = pl.DeviceIdType.MESH

first_decay = 0.9
second_decay = 0.95
divide_guard = 1e-08
mean_guard = 1e-06
clip_level = 0.1


def groups_of(nz):
    return min(4, nz // 2)


def permutation(nz, nx, base):
    n = 2 * nz * nx
    pairs = nz // 2
    E = pairs // groups_of(nz)
    p = lax.broadcasted_iota(jnp.int32, (n, n), 0)
    r = lax.broadcasted_iota(jnp.int32, (n, n), 1)
    log = lambda v: v.bit_length() - 1
    shift, mask = lax.shift_right_logical, lax.bitwise_and
    k = shift(p, log(4 * E * nx)) * E + mask(shift(p, 1), E - 1)
    parity = mask(shift(p, log(2 * E)), 1)
    px = mask(shift(p, log(4 * E)), nx - 1)
    reach = pairs // 2 - shift(k + 1, 1)
    offset = jnp.where(mask(k, 1) == 1, reach, -reach)
    target = mask(base + nz + 2 * offset + parity, nz - 1)
    want = target * (2 * nx) + 2 * px + mask(p, 1)
    return jnp.where(want == r, 1.0, 0.0).astype(jnp.bfloat16)


def dot_t(a, b):
    return lax.dot_general(a, b, (((1,), (1,)), ((), ())), preferred_element_type=jnp.float32)


def exchange(
    nz, nx, ny,
    a0, u0, u1, a1, l0, l1, m0, m1, s0, s1,
    out_step, out_fs, out_q,
    X, F, U, PS, CR, S, XR, TP, PR, ZS, ZR, ZG, HX, MS, MR, FO, QY, QZ, QP, ST,
    load_sem, small_sem, core_send, core_recv, x_send, x_recv, p_send, p_recv,
    z_send, z_recv, g_recv, h_send, h_recv, q_send, q_recv, ready,
):
    z = lax.axis_index("fs_0")
    x = lax.axis_index("fs_1")
    c = lax.axis_index("fs_2")
    y = lax.axis_index("tp")
    other = 1 - c
    W = u0.shape[1]
    tokens = a0.shape[0] // 2
    NG = groups_of(nz)
    NP = nz // 2
    E = NP // NG
    HR = 2 * E
    GR = 2 * HR
    b = lax.rem(z, 2)
    base = z - b
    twin = base + 1 - b
    reach = max(2, nz // 8)

    def z_at(offset):
        return lax.rem(z + nz + offset, nz)

    def z_target(k):
        far = NP // 2 - lax.div(k + 1, 2)
        return z_at(2 * far * (2 * lax.rem(k, 2) - 1))

    def around(j):
        return {
            "fs_0": base + lax.rem(b + lax.rem(lax.div(j, nx), 2), 2),
            "fs_1": lax.rem(x + lax.rem(j, nx), nx),
            "fs_2": lax.rem(c + lax.div(j, 2 * nx), 2),
        }

    with jax.named_scope("p00_loads"):
        sources = ((l0, a0, u0), (l1, a1, u1))
        halves = (pl.ds(0, tokens), pl.ds(tokens, tokens))

        def parts(m):
            l, a, u = sources[m]
            return (
                (l, F.at[m]), (a.at[halves[0]], X.at[m, 0]), (a.at[halves[1]], X.at[m, 1]), (u, U.at[m]),
            )

        for mine in range(2):

            @pl.when(c == mine)
            def _(mine=mine):
                for m in (1 - mine, mine):
                    for k, (src, dst) in enumerate(parts(m)):
                        pltpu.make_async_copy(src, dst, load_sem.at[m, k]).start()

        small = []
        for k, (src, dst) in enumerate((
            (m0, MS.at[0, 0]), (s0, MS.at[0, 1]), (m1, MS.at[1, 0]), (s1, MS.at[1, 1]),
        )):
            cp = pltpu.make_async_copy(src, dst, small_sem.at[k])
            cp.start()
            small.append(cp)

    with jax.named_scope("p01_greet"):
        barrier = pltpu.get_barrier_semaphore()
        met = 0
        for d in range(reach, 0, -2):
            for offset in (d, -d):
                pl.semaphore_signal(barrier, inc=1, device_id={"fs_0": z_at(offset)}, device_id_type=MESH)
                met += 1
        for d in range(1, ny):
            pl.semaphore_signal(barrier, inc=1, device_id={"tp": lax.rem(y + d, ny)}, device_id_type=MESH)
            met += 1

        def greet(j, carry):
            pl.semaphore_signal(barrier, inc=1, device_id=around(j), device_id_type=MESH)
            return carry

        lax.fori_loop(1, 4 * nx, greet, 0)
        met += 4 * nx - 1

    perm = permutation(nz, nx, base)

    def arrived(m, k):
        src, dst = parts(0)[k]
        dst = (F.at[m], X.at[m, 0], X.at[m, 1], U.at[m])[k]
        pltpu.make_async_copy(src, dst, load_sem.at[m, k]).wait()

    def project(m):
        arrived(m, 0)
        turned = []
        for h in range(2):
            arrived(m, 1 + h)
            rows = jnp.dot(X[m, h], F[m], preferred_element_type=jnp.float32).astype(jnp.bfloat16)
            turned.append(dot_t(perm, rows).astype(jnp.bfloat16))
        arrived(m, 3)
        sums = jnp.dot(jnp.concatenate(turned, axis=1), U[m], preferred_element_type=jnp.float32)
        PS[m] = sums.reshape(NG, nx * GR, W)

    def remote(src, dst, send, recv, **where):
        return pltpu.make_async_remote_copy(
            src_ref=src, dst_ref=dst, send_sem=send, recv_sem=recv, device_id=where, device_id_type=MESH
        )

    with jax.named_scope("p02_project"):
        project(other)
        for cp in small:
            cp.wait()
    with jax.named_scope("p03_barrier"):
        pl.semaphore_wait(barrier, met)

    for offset in (reach, -reach):
        pl.semaphore_signal(ready.at[0], inc=1, device_id={"fs_0": z_at(offset)}, device_id_type=MESH)

    give = [
        remote(PS.at[other, g], CR.at[g], core_send.at[g], core_recv.at[g], fs_2=other) for g in range(NG)
    ]
    for cp in give:
        cp.start()
    give_m = remote(MS.at[other], MR, core_send.at[NG], core_recv.at[NG], fs_2=other)
    give_m.start()
    with jax.named_scope("p04_project"):
        project(c)

    x_order = (2, 1, 3)
    with jax.named_scope("p05_xsend"):
        for g in range(NG):
            give[g].wait_recv()
            S[g] = (PS[c, g] + CR[g]).reshape(nx, GR, W)
            for d in x_order:
                t = lax.rem(x + d, nx)
                remote(S.at[g, t], XR.at[g, d - 1], x_send.at[0], x_recv.at[g], fs_1=t).start()

    with jax.named_scope("p06_ready"):
        pl.semaphore_wait(ready.at[0], 2)
        for offset in (2 * reach, -2 * reach):
            pl.semaphore_signal(ready.at[1], inc=1, device_id={"fs_0": z_at(offset)}, device_id_type=MESH)

    next_x = lax.rem(x + 1, nx)
    next_z = z_at(2)

    def sum_x(g):
        with jax.named_scope(f"p07_x{g}"):
            remote(XR.at[g], XR.at[g], x_send.at[0], x_recv.at[g], fs_1=next_x).wait_recv()
            part = S[g, x] + (XR[g, 0] + XR[g, 1] + XR[g, 2])
            TP[g] = part.reshape(2, HR, W)
            remote(TP.at[g, 1 - b], PR.at[g], p_send.at[0], p_recv.at[g], fs_0=twin).start()

    def scatter(k, carry):
        remote(ZS.at[k], ZR.at[k], z_send.at[0], z_recv.at[0], fs_0=z_target(k)).start()
        return carry

    def sum_twin(g):
        with jax.named_scope(f"p08_t{g}"):
            remote(PR.at[g], PR.at[g], p_send.at[0], p_recv.at[g], fs_0=twin).wait_recv()
            part = TP[g, b] + PR[g]
            for e in range(E):
                ZS[g * E + e] = part[2 * e : 2 * e + 2]
            if g == 0:
                pl.semaphore_wait(ready.at[1], 2)
            lax.fori_loop(g * E, min((g + 1) * E, NP - 1), scatter, 0)

    for g in range(NG):
        sum_x(g)
        if g > 0:
            sum_twin(g - 1)
    sum_twin(NG - 1)
    with jax.named_scope("p09_zwait"):
        all_in = remote(ZR, ZR, z_send.at[0], z_recv.at[0], fs_0=next_z)
        all_in.wait_recv()
    with jax.named_scope("p10_moment"):
        proj = ZS[NP - 1] + jnp.sum(ZR[...], axis=0)
        give_m.wait_recv()

        def both(own, got):
            top = jnp.where(c == 0, own, got)
            low = jnp.where(c == 0, got, own)
            return jnp.concatenate([top, low], axis=0)

        moment = both(MS[c, 0], MR[0])
        square = both(MS[c, 1], MR[1])
        first = first_decay * moment + (1.0 - first_decay) * proj
        second = second_decay * square + (1.0 - second_decay) * proj * proj
        heading = first / (jnp.sqrt(second) + divide_guard)
        ZG[NP - 1] = heading

    def slot_of(k):
        return jnp.where(k == 0, 0, k + 2 * lax.rem(k, 2) - 1)

    def spread(k, carry):
        slot = slot_of(k)
        remote(ZG.at[NP - 1], ZG.at[slot], z_send.at[1], g_recv.at[lax.div(slot, E)], fs_0=z_target(k)).start()
        return carry

    with jax.named_scope("p11_zsend"):
        lax.fori_loop(0, NP - 1, spread, 0)

    with jax.named_scope("p12_squares"):
        wide = heading * heading
        row = wide[:, 0:128]
        for k in range(128, W, 128):
            row = row + wide[:, k : k + 128]
        QY[0] = jnp.sum(row, axis=0, keepdims=True)
        for d in range(1, ny):
            remote(QY.at[0], QY.at[d], q_send.at[0], q_recv.at[0], tp=lax.rem(y + d, ny)).start()

        out_fs[c, 0] = jnp.where(c == 0, first[0:1], first[1:2])
        out_fs[c, 1] = jnp.where(c == 0, second[0:1], second[1:2])
        FO[0] = jnp.where(c == 0, first[1:2], first[0:1])
        FO[1] = jnp.where(c == 0, second[1:2], second[0:1])
        give_f = remote(FO, out_fs.at[c], core_send.at[NG + 1], core_recv.at[NG + 1], fs_2=other)
        give_f.start()
        start = pl.multiple_of((z * nx + x) * 16, 16)
        factor = dot_t(F[c, pl.ds(start, 16), :], perm)
        if ny > 1:
            y_all = remote(
                QY.at[pl.ds(1, ny - 1)], QY.at[pl.ds(1, ny - 1)], q_send.at[0], q_recv.at[0], fs_0=next_z
            )
            y_all.wait_recv()
        QZ[NP - 1] = jnp.sum(QY[...], axis=0)

        def spread_q(k, carry):
            remote(QZ.at[NP - 1], QZ.at[slot_of(k)], q_send.at[1], q_recv.at[1], fs_0=z_target(k)).start()
            return carry

        lax.fori_loop(0, NP - 1, spread_q, 0)

    def to_x(g, parity):
        for d in x_order:
            t = lax.rem(x + d, nx)
            remote(HX.at[g, x, parity], HX.at[g, x, parity], h_send.at[0], h_recv.at[g], fs_1=t).start()

    def forward(g):
        with jax.named_scope(f"p13_z{g}"):
            count = min((g + 1) * E, NP - 1) - g * E
            if count:
                remote(
                    ZR.at[pl.ds(0, count)], ZR.at[pl.ds(0, count)], z_send.at[1], g_recv.at[g], fs_0=next_z
                ).wait_recv()
        for e in range(E):
            HX[g, x, b, 2 * e : 2 * e + 2] = ZG[g * E + e]
        remote(HX.at[g, x, b], HX.at[g, x, b], p_send.at[1], p_recv.at[NG + g], fs_0=twin).start()
        to_x(g, b)

    def forward_twin(g):
        with jax.named_scope(f"p14_t{g}"):
            remote(PR.at[g], PR.at[g], p_send.at[1], p_recv.at[NG + g], fs_0=twin).wait_recv()
        to_x(g, 1 - b)

    block = jnp.zeros((16, W), jnp.float32)

    def times(g, block):
        with jax.named_scope(f"p15_x{g}"):
            remote(XR.at[g], XR.at[g], h_send.at[0], h_recv.at[g], fs_1=next_x).wait_recv()
        return block + jnp.dot(
            factor[:, g * nx * GR : (g + 1) * nx * GR], HX[g].reshape(nx * GR, W),
            precision=lax.Precision.HIGHEST, preferred_element_type=jnp.float32,
        )

    order = list(reversed(range(NG)))
    for i, g in enumerate(order):
        forward(g)
        if i > 0:
            forward_twin(order[i - 1])
    with jax.named_scope("p16_q"):
        z_told = remote(
            QZ.at[pl.ds(0, NP - 1)], QZ.at[pl.ds(0, NP - 1)], q_send.at[1], q_recv.at[1], fs_0=next_z
        )
        z_told.wait_recv()
        QP[0] = jnp.sum(QZ[...], axis=0)

        def tell(j, carry):
            remote(QP.at[0], QP.at[j], q_send.at[2], q_recv.at[2], **around(j)).start()
            return carry

        lax.fori_loop(1, 4 * nx, tell, 0)
    forward_twin(order[-1])
    for g in order:
        block = times(g, block)
    ST[...] = block.reshape(2, 8, W)
    give_s = remote(ST.at[other], out_step.at[c], core_send.at[NG + 2], core_recv.at[NG + 2], fs_2=other)
    give_s.start()
    out_step[c] = ST[c]
    with jax.named_scope("p17_q"):
        told = QP.at[pl.ds(1, 4 * nx - 1)]
        q_all = remote(told, told, q_send.at[2], q_recv.at[2], fs_1=next_x)
        q_all.wait_recv()
        out_q[c] = jnp.sum(QP[0 : 2 * nx], axis=0)
        out_q[other] = jnp.sum(QP[2 * nx : 4 * nx], axis=0)

    with jax.named_scope("p18_drain"):
        for cp in (*give, give_m):
            cp.wait_send()
        remote(XR, XR, x_send.at[0], x_recv.at[0], fs_1=next_x).wait_send()
        for k in range(2):
            remote(PR, PR, p_send.at[k], p_recv.at[0], fs_0=twin).wait_send()
        all_in.wait_send()
        remote(ZR, ZR, z_send.at[1], g_recv.at[0], fs_0=next_z).wait_send()
        remote(XR, XR, h_send.at[0], h_recv.at[0], fs_1=next_x).wait_send()
        if ny > 1:
            y_all.wait_send()
        z_told.wait_send()
        q_all.wait_send()
        give_f.wait()
        give_s.wait()


def finish(entries, step, fs, q, mi, mo, fi, fo, si, so, ti, to, wi, wo, ci, co):
    fi[...] = fs[0, 0]
    si[...] = fs[0, 1]
    fo[...] = fs[1, 0]
    so[...] = fs[1, 1]
    for m, (old, out, new, copy) in enumerate(((mi, ti, wi, ci), (mo, to, wo, co))):
        mean = jnp.sum(q[m], axis=1, keepdims=True) / entries
        gain = jnp.minimum(1.0, clip_level / jnp.sqrt(mean + mean_guard))
        s = gain * step[m]
        out[...] = s
        w = old[...] - s
        new[...] = w
        copy[...] = w.astype(jnp.bfloat16)


def shards(nz, nx, ny, saved, unit, gated, mixer, left, right, mi, mo, m0, m1, s0, s1):
    f32, bf16 = jnp.float32, jnp.bfloat16
    n, d = saved.shape
    W = unit.shape[1]
    rank = left.shape[1]
    assert rank == 2 * nz * nx and nx == 4 and mi.shape[0] == 8 and m0.shape[0] == 1
    entries = float(rank * W * ny)
    V = pltpu.VMEM
    dma = pltpu.SemaphoreType.DMA
    NG, NP = groups_of(nz), nz // 2
    HR = 2 * NP // NG
    GR = 2 * HR
    anywhere = pl.BlockSpec(memory_space=pl.ANY)
    vmem = pl.BlockSpec(memory_space=pltpu.VMEM)
    step, fs, q = pl.pallas_call(
        functools.partial(exchange, nz, nx, ny),
        out_shape=(
            jax.ShapeDtypeStruct((2, 8, W), f32),
            jax.ShapeDtypeStruct((2, 2, 1, W), f32),
            jax.ShapeDtypeStruct((2, 1, 128), f32),
        ),
        in_specs=[anywhere] * 10,
        out_specs=(vmem, vmem, vmem),
        scratch_shapes=[
            V((2, 2, n // 2, d), bf16),
            V((2, d, rank), bf16),
            V((2, n, W), bf16),
            V((2, NG, nx * GR, W), f32),
            V((NG, nx * GR, W), f32),
            V((NG, nx, GR, W), f32),
            V((NG, nx - 1, GR, W), f32),
            V((NG, 2, HR, W), f32),
            V((NG, HR, W), f32),
            V((NP, 2, W), f32),
            V((NP - 1, 2, W), f32),
            V((NP, 2, W), f32),
            V((NG, nx, 2, HR, W), f32),
            V((2, 2, 1, W), f32),
            V((2, 1, W), f32),
            V((2, 1, W), f32),
            V((ny, 1, 128), f32),
            V((NP, 1, 128), f32),
            V((4 * nx, 1, 128), f32),
            V((2, 8, W), f32),
            dma((2, 4)),
            dma((4,)),
            dma((NG + 3,)),
            dma((NG + 3,)),
            dma((1,)),
            dma((NG,)),
            dma((2,)),
            dma((2 * NG,)),
            dma((2,)),
            dma((1,)),
            dma((NG,)),
            dma((1,)),
            dma((NG,)),
            dma((3,)),
            dma((3,)),
            pltpu.SemaphoreType.REGULAR((2,)),
        ],
        compiler_params=pltpu.CompilerParams(collective_id=0, has_side_effects=True),
        name="exchange",
    )(saved, unit, gated, mixer, left, right, m0, m1, s0, s1)
    row = jax.ShapeDtypeStruct((1, W), f32)
    wide = jax.ShapeDtypeStruct((8, W), f32)
    short = jax.ShapeDtypeStruct((8, W), bf16)
    outs = pl.pallas_call(
        functools.partial(finish, entries),
        out_shape=(row, row, row, row, wide, wide, wide, wide, short, short),
        name="finish",
    )(step, fs, q, mi, mo.T)
    return tuple(out.T if k in (5, 7, 9) else out for k, out in enumerate(outs))


def solution(mesh):
    ny = mesh.shape["tp"]
    nx = 4
    nz = mesh.shape["fs"] // (2 * nx)
    finer = Mesh(mesh.devices.reshape(nz, nx, 2, ny), (*FS, "tp"))
    rows, cols = P(FS, "tp"), P("tp", FS)
    return jax.shard_map(
        functools.partial(shards, nz, nx, ny),
        mesh=finer,
        in_specs=(P(FS, None), rows, rows, P(FS, None), P(), P(), rows, cols, rows, rows, rows, rows),
        out_specs=(rows, rows, rows, rows, rows, cols, rows, cols, rows, cols),
        check_vma=False,
    )
```

time: 606 us -> 70.4 us (0.12)
  waiting for transfers between devices: 327 us -> 0 us
  blocking collectives: 236 us -> 0 us
  Pallas kernels: 0 us -> 69.6 us
  between operations: 15.2 us -> 0.65 us
  local copies, waits for them, and re-layouts: 12.8 us -> 0 us
  matrix products: 10.9 us -> 0 us
    unnamed x4 -> x0, waiting for transfers between devices: 246 us -> none
    all_gather x6 -> x0, blocking collectives: 137 us -> none  [all_blocks(): pieces = lax.all_gather(pieces, axes[k], axis=0, tiled=True)]
    psum x4 -> x0, blocking collectives: 99.9 us -> none  [by_axis(): return functools.reduce(lax.psum, axes, array)]
    reduce_scatter x2 -> x0, waiting for transfers between devices: 80.9 us -> none  [own_block(): pieces = lax.psum_scatter(pieces, axes[k], scatter_dimension=0, tiled=True)]
    pallas_call x0 -> x2, Pallas kernels: none -> 69.6 us  [the longest x1 68 us: shards(): pl.pallas_call(functools.partial(exchange, nz, nx, ny), out_shape=(jax.Sh...]
    dot_general x4 -> x0, matrix products: 10.9 us -> none  [the longest x2 7.59 us: contract_tokens(): lax.dot_general(left, right, (((0,), (0,)), ((), ())), preferred_element_...]
    another operation x4 -> x0, local copies, waits for them, and re-layouts: 6.7 us -> none  [the longest x2 4.71 us: own_block(): pieces = pieces.reshape(*(lax.axis_size(a) for a in axes), *inside)]
  transfers between devices with their start and end apart: 3 -> 0, of which waited for: 3 -> 0; matrix products, arithmetic and copies ran while one was open for 0% -> 0% of each run, Pallas kernels for 0% -> 0%
where the time goes in v2:
time: 70.4 us; the launch traced here: 70.2 us
  Pallas kernels  69.6 us (99%)
    pallas_call x1, Pallas kernels, shards(): pl.pallas_call(functools.partial(exchange, nz, nx, ny), out_shape=(jax.Sh...  68 us
    pallas_call x1, Pallas kernels, shards(): pl.pallas_call(functools.partial(finish, entries), out_shape=(row, row, r...  1.55 us

profile of v2, /device:TPU:1, one launch (start us, length us, event | category | flops | bytes accessed | tf_op | source)
XLA Modules:
  0.0 70.2 jit_solution(7988167608415762148)
XLA Ops:
  0.6 68.0 %exchange.1 = (f32[2,8,640]{2,1,0:T(8,128)}, f32[2,2,1,640]{3,2,1,0:T(1,128)}, f32[2,1,128]{2,1,0:T(1,128)}) custom-call(bf16[512,2048]{1,0:T(8,128)(2,1)} %a0.1, bf16[512,640]{1,0:T(8,128)(2,1)} %u0.1, bf16[512,640]{1,0:T(8,128)(2,1)} %u1_.1, bf16[512,2048]{1,0:T(8,128)(2,1)} %a1.1, bf16[2048,256]{1,0:T(8,128)(2,1)} %l0.1, bf16[2048,256]{1,0:T(8,128)(2,1)} %l1.1, ...), custom_call_target="tpu_custom_call" | custom-call | tf_op jit(solution)/shard_map/exchange/pallas_call | solution.py:385
  68.7 1.6 %finish.1 = (f32[1,640]{1,0:T(1,128)}, f32[1,640]{1,0:T(1,128)}, f32[1,640]{1,0:T(1,128)}, f32[1,640]{1,0:T(1,128)}, f32[8,640]{1,0:T(8,128)}, /*index=5*/f32[8,...) custom-call(f32[2,8,640]{2,1,0:T(8,128)} %get-tuple-element.23.step, ...), custom_call_target="tpu_custom_call" | custom-call | tf_op jit(solution)/shard_map/finish/pallas_call | solution.py:438

commit v3 on v2

--- a/solution.py
+++ b/solution.py
@@ -46,9 +46,9 @@
 
 def exchange(
     nz, nx, ny,
-    a0, u0, u1, a1, l0, l1, m0, m1, s0, s1,
-    out_step, out_fs, out_q,
-    X, F, U, PS, CR, S, XR, TP, PR, ZS, ZR, ZG, HX, MS, MR, FO, QY, QZ, QP, ST,
+    a0, u0, u1, a1, l0, l1, m0, m1, s0, s1, w0, w1,
+    out_step, out_fs, out_q, out_old,
+    X, F, FP, RW, U, PS, CR, S, XR, TP, PR, ZS, ZR, ZG, HX, MS, MR, FO, QP, ST, FC,
     load_sem, small_sem, core_send, core_recv, x_send, x_recv, p_send, p_recv,
     z_send, z_recv, g_recv, h_send, h_recv, q_send, q_recv, ready,
 ):
@@ -73,8 +73,8 @@
         return lax.rem(z + nz + offset, nz)
 
     def z_target(k):
-        far = NP // 2 - lax.div(k + 1, 2)
-        return z_at(2 * far * (2 * lax.rem(k, 2) - 1))
+        far = NP // 2 - (k + 1) // 2
+        return z_at(2 * far * (2 * (k % 2) - 1))
 
     def around(j):
         return {
@@ -97,13 +97,13 @@
 
             @pl.when(c == mine)
             def _(mine=mine):
-                for m in (1 - mine, mine):
-                    for k, (src, dst) in enumerate(parts(m)):
-                        pltpu.make_async_copy(src, dst, load_sem.at[m, k]).start()
+                for m, k in [(m, k) for ks in ((0,), (1, 2, 3)) for m in (1 - mine, mine) for k in ks]:
+                    src, dst = parts(m)[k]
+                    pltpu.make_async_copy(src, dst, load_sem.at[m, k]).start()
 
         small = []
         for k, (src, dst) in enumerate((
-            (m0, MS.at[0, 0]), (s0, MS.at[0, 1]), (m1, MS.at[1, 0]), (s1, MS.at[1, 1]),
+            (m0, MS.at[0, 0]), (s0, MS.at[0, 1]), (m1, MS.at[1, 0]), (s1, MS.at[1, 1]), (w0, out_old.at[0]), (w1, out_old.at[1]),
         )):
             cp = pltpu.make_async_copy(src, dst, small_sem.at[k])
             cp.start()
@@ -135,14 +135,13 @@
         pltpu.make_async_copy(src, dst, load_sem.at[m, k]).wait()
 
     def project(m):
-        arrived(m, 0)
-        turned = []
         for h in range(2):
             arrived(m, 1 + h)
-            rows = jnp.dot(X[m, h], F[m], preferred_element_type=jnp.float32).astype(jnp.bfloat16)
-            turned.append(dot_t(perm, rows).astype(jnp.bfloat16))
+            RW[halves[h]] = jnp.dot(X[m, h], FP[m], preferred_element_type=jnp.float32).astype(jnp.bfloat16)
         arrived(m, 3)
-        sums = jnp.dot(jnp.concatenate(turned, axis=1), U[m], preferred_element_type=jnp.float32)
+        sums = lax.dot_general(
+            RW[...], U[m], (((0,), (0,)), ((), ())), preferred_element_type=jnp.float32
+        )
         PS[m] = sums.reshape(NG, nx * GR, W)
 
     def remote(src, dst, send, recv, **where):
@@ -150,6 +149,10 @@
             src_ref=src, dst_ref=dst, send_sem=send, recv_sem=recv, device_id=where, device_id_type=MESH
         )
 
+    with jax.named_scope("p02_factors"):
+        for m in (other, c):
+            arrived(m, 0)
+            FP[m] = dot_t(F[m], perm).astype(jnp.bfloat16)
     with jax.named_scope("p02_project"):
         project(other)
         for cp in small:
@@ -159,6 +162,8 @@
 
     for offset in (reach, -reach):
         pl.semaphore_signal(ready.at[0], inc=1, device_id={"fs_0": z_at(offset)}, device_id_type=MESH)
+    for d in range(1, ny):
+        pl.semaphore_signal(ready.at[0], inc=1, device_id={"tp": lax.rem(y + d, ny)}, device_id_type=MESH)
 
     give = [
         remote(PS.at[other, g], CR.at[g], core_send.at[g], core_recv.at[g], fs_2=other) for g in range(NG)
@@ -180,7 +185,7 @@
                 remote(S.at[g, t], XR.at[g, d - 1], x_send.at[0], x_recv.at[g], fs_1=t).start()
 
     with jax.named_scope("p06_ready"):
-        pl.semaphore_wait(ready.at[0], 2)
+        pl.semaphore_wait(ready.at[0], 1 + ny)
         for offset in (2 * reach, -2 * reach):
             pl.semaphore_signal(ready.at[1], inc=1, device_id={"fs_0": z_at(offset)}, device_id_type=MESH)
 
@@ -193,10 +198,6 @@
             part = S[g, x] + (XR[g, 0] + XR[g, 1] + XR[g, 2])
             TP[g] = part.reshape(2, HR, W)
             remote(TP.at[g, 1 - b], PR.at[g], p_send.at[0], p_recv.at[g], fs_0=twin).start()
-
-    def scatter(k, carry):
-        remote(ZS.at[k], ZR.at[k], z_send.at[0], z_recv.at[0], fs_0=z_target(k)).start()
-        return carry
 
     def sum_twin(g):
         with jax.named_scope(f"p08_t{g}"):
@@ -206,7 +207,8 @@
                 ZS[g * E + e] = part[2 * e : 2 * e + 2]
             if g == 0:
                 pl.semaphore_wait(ready.at[1], 2)
-            lax.fori_loop(g * E, min((g + 1) * E, NP - 1), scatter, 0)
+            for k in range(g * E, min((g + 1) * E, NP - 1)):
+                remote(ZS.at[k], ZR.at[k], z_send.at[0], z_recv.at[0], fs_0=z_target(k)).start()
 
     for g in range(NG):
         sum_x(g)
@@ -232,26 +234,12 @@
         heading = first / (jnp.sqrt(second) + divide_guard)
         ZG[NP - 1] = heading
 
-    def slot_of(k):
-        return jnp.where(k == 0, 0, k + 2 * lax.rem(k, 2) - 1)
-
-    def spread(k, carry):
-        slot = slot_of(k)
-        remote(ZG.at[NP - 1], ZG.at[slot], z_send.at[1], g_recv.at[lax.div(slot, E)], fs_0=z_target(k)).start()
-        return carry
-
     with jax.named_scope("p11_zsend"):
-        lax.fori_loop(0, NP - 1, spread, 0)
-
-    with jax.named_scope("p12_squares"):
-        wide = heading * heading
-        row = wide[:, 0:128]
-        for k in range(128, W, 128):
-            row = row + wide[:, k : k + 128]
-        QY[0] = jnp.sum(row, axis=0, keepdims=True)
-        for d in range(1, ny):
-            remote(QY.at[0], QY.at[d], q_send.at[0], q_recv.at[0], tp=lax.rem(y + d, ny)).start()
-
+        for k in range(NP - 1):
+            slot = k + 2 * (k % 2) - 1 if k else 0
+            remote(ZG.at[NP - 1], ZG.at[slot], z_send.at[1], g_recv.at[slot // E], fs_0=z_target(k)).start()
+
+    with jax.named_scope("p12_owner"):
         out_fs[c, 0] = jnp.where(c == 0, first[0:1], first[1:2])
         out_fs[c, 1] = jnp.where(c == 0, second[0:1], second[1:2])
         FO[0] = jnp.where(c == 0, first[1:2], first[0:1])
@@ -259,26 +247,16 @@
         give_f = remote(FO, out_fs.at[c], core_send.at[NG + 1], core_recv.at[NG + 1], fs_2=other)
         give_f.start()
         start = pl.multiple_of((z * nx + x) * 16, 16)
-        factor = dot_t(F[c, pl.ds(start, 16), :], perm)
-        if ny > 1:
-            y_all = remote(
-                QY.at[pl.ds(1, ny - 1)], QY.at[pl.ds(1, ny - 1)], q_send.at[0], q_recv.at[0], fs_0=next_z
-            )
-            y_all.wait_recv()
-        QZ[NP - 1] = jnp.sum(QY[...], axis=0)
-
-        def spread_q(k, carry):
-            remote(QZ.at[NP - 1], QZ.at[slot_of(k)], q_send.at[1], q_recv.at[1], fs_0=z_target(k)).start()
-            return carry
-
-        lax.fori_loop(0, NP - 1, spread_q, 0)
+        factor = FP[c, pl.ds(start, 16), :]
+        for g in range(NG):
+            FC[g] = factor[:, g * nx * GR : (g + 1) * nx * GR]
 
     def to_x(g, parity):
         for d in x_order:
             t = lax.rem(x + d, nx)
             remote(HX.at[g, x, parity], HX.at[g, x, parity], h_send.at[0], h_recv.at[g], fs_1=t).start()
 
-    def forward(g):
+    def forward(g, squares):
         with jax.named_scope(f"p13_z{g}"):
             count = min((g + 1) * E, NP - 1) - g * E
             if count:
@@ -286,55 +264,78 @@
                     ZR.at[pl.ds(0, count)], ZR.at[pl.ds(0, count)], z_send.at[1], g_recv.at[g], fs_0=next_z
                 ).wait_recv()
         for e in range(E):
-            HX[g, x, b, 2 * e : 2 * e + 2] = ZG[g * E + e]
+            piece = ZG[g * E + e]
+            HX[g, x, b, 2 * e : 2 * e + 2] = piece
+            piece = piece * piece
+            for k in range(0, W, 128):
+                squares = squares + piece[:, k : k + 128]
         remote(HX.at[g, x, b], HX.at[g, x, b], p_send.at[1], p_recv.at[NG + g], fs_0=twin).start()
         to_x(g, b)
+        if g == 0:
+            for d in x_order:
+                t = lax.rem(x + d, nx)
+                remote(
+                    HX.at[g, x, b], HX.at[g, x, b], h_send.at[0], h_recv.at[g], fs_0=twin, fs_1=t
+                ).start()
+            QP[0] = jnp.sum(squares, axis=0, keepdims=True)
+            tell()
+        return squares
+
+    crowd = 4 * nx * ny
+
+    def tell():
+        sides = [lax.rem(x + d, nx) for d in range(nx)]
+        ups = [lax.rem(y + d, ny) for d in range(ny)]
+        for dy in sorted(range(ny), key=lambda d: -min(d, ny - d)):
+            for dx in sorted(range(nx), key=lambda d: -min(d, nx - d)):
+                for db in (1, 0):
+                    for dc in (1, 0):
+                        slot = dc * (crowd // 2) + (db * ny + dy) * nx + dx
+                        if slot:
+                            remote(
+                                QP.at[0], QP.at[slot], q_send.at[0], q_recv.at[0],
+                                fs_0=(z, twin)[db], fs_1=sides[dx], fs_2=(c, other)[dc], tp=ups[dy],
+                            ).start()
 
     def forward_twin(g):
         with jax.named_scope(f"p14_t{g}"):
             remote(PR.at[g], PR.at[g], p_send.at[1], p_recv.at[NG + g], fs_0=twin).wait_recv()
-        to_x(g, 1 - b)
-
-    block = jnp.zeros((16, W), jnp.float32)
-
-    def times(g, block):
-        with jax.named_scope(f"p15_x{g}"):
-            remote(XR.at[g], XR.at[g], h_send.at[0], h_recv.at[g], fs_1=next_x).wait_recv()
+        if g > 0:
+            to_x(g, 1 - b)
+
+    squares = jnp.zeros((2, 128), jnp.float32)
+    for g in reversed(range(NG)):
+        squares = forward(g, squares)
+        if g < NG - 1:
+            forward_twin(g + 1)
+    forward_twin(0)
+
+    def times(i, block):
+        g = NG - 1 - i
+        remote(XR.at[g], XR.at[g], h_send.at[0], h_recv.at[g], fs_1=next_x).wait_recv()
+        whole = HX[g].reshape(nx * GR, W)
+        high = whole.astype(jnp.bfloat16)
+        rest = whole - high.astype(jnp.float32)
+        middle = rest.astype(jnp.bfloat16)
+        low = (rest - middle.astype(jnp.float32)).astype(jnp.bfloat16)
+        part = FC[g]
         return block + jnp.dot(
-            factor[:, g * nx * GR : (g + 1) * nx * GR], HX[g].reshape(nx * GR, W),
-            precision=lax.Precision.HIGHEST, preferred_element_type=jnp.float32,
+            jnp.concatenate([part, part, part], axis=1), jnp.concatenate([low, middle, high], axis=0),
+            preferred_element_type=jnp.float32,
         )
 
-    order = list(reversed(range(NG)))
-    for i, g in enumerate(order):
-        forward(g)
-        if i > 0:
-            forward_twin(order[i - 1])
-    with jax.named_scope("p16_q"):
-        z_told = remote(
-            QZ.at[pl.ds(0, NP - 1)], QZ.at[pl.ds(0, NP - 1)], q_send.at[1], q_recv.at[1], fs_0=next_z
-        )
-        z_told.wait_recv()
-        QP[0] = jnp.sum(QZ[...], axis=0)
-
-        def tell(j, carry):
-            remote(QP.at[0], QP.at[j], q_send.at[2], q_recv.at[2], **around(j)).start()
-            return carry
-
-        lax.fori_loop(1, 4 * nx, tell, 0)
-    forward_twin(order[-1])
-    for g in order:
-        block = times(g, block)
+    with jax.named_scope("p15_x"):
+        block = lax.fori_loop(0, NG, times, jnp.zeros((16, W), jnp.float32))
     ST[...] = block.reshape(2, 8, W)
     give_s = remote(ST.at[other], out_step.at[c], core_send.at[NG + 2], core_recv.at[NG + 2], fs_2=other)
     give_s.start()
     out_step[c] = ST[c]
     with jax.named_scope("p17_q"):
-        told = QP.at[pl.ds(1, 4 * nx - 1)]
-        q_all = remote(told, told, q_send.at[2], q_recv.at[2], fs_1=next_x)
+        told = QP.at[pl.ds(1, crowd - 1)]
+        q_all = remote(told, told, q_send.at[0], q_recv.at[0], fs_1=next_x)
         q_all.wait_recv()
-        out_q[c] = jnp.sum(QP[0 : 2 * nx], axis=0)
-        out_q[other] = jnp.sum(QP[2 * nx : 4 * nx], axis=0)
+        out_q[c] = jnp.sum(QP[0 : crowd // 2], axis=0)
+        out_q[other] = jnp.sum(QP[crowd // 2 : crowd], axis=0)
 
     with jax.named_scope("p18_drain"):
         for cp in (*give, give_m):
@@ -345,25 +346,22 @@
         all_in.wait_send()
         remote(ZR, ZR, z_send.at[1], g_recv.at[0], fs_0=next_z).wait_send()
         remote(XR, XR, h_send.at[0], h_recv.at[0], fs_1=next_x).wait_send()
-        if ny > 1:
-            y_all.wait_send()
-        z_told.wait_send()
         q_all.wait_send()
         give_f.wait()
         give_s.wait()
 
 
-def finish(entries, step, fs, q, mi, mo, fi, fo, si, so, ti, to, wi, wo, ci, co):
+def finish(entries, step, fs, q, old, fi, fo, si, so, ti, to, wi, wo, ci, co):
     fi[...] = fs[0, 0]
     si[...] = fs[0, 1]
     fo[...] = fs[1, 0]
     so[...] = fs[1, 1]
-    for m, (old, out, new, copy) in enumerate(((mi, ti, wi, ci), (mo, to, wo, co))):
+    for m, (out, new, copy) in enumerate(((ti, wi, ci), (to, wo, co))):
         mean = jnp.sum(q[m], axis=1, keepdims=True) / entries
         gain = jnp.minimum(1.0, clip_level / jnp.sqrt(mean + mean_guard))
         s = gain * step[m]
         out[...] = s
-        w = old[...] - s
+        w = old[m] - s
         new[...] = w
         copy[...] = w.astype(jnp.bfloat16)
 
@@ -382,18 +380,21 @@
     GR = 2 * HR
     anywhere = pl.BlockSpec(memory_space=pl.ANY)
     vmem = pl.BlockSpec(memory_space=pltpu.VMEM)
-    step, fs, q = pl.pallas_call(
+    step, fs, q, old = pl.pallas_call(
         functools.partial(exchange, nz, nx, ny),
         out_shape=(
-            jax.ShapeDtypeStruct((2, 8, W), f32),
-            jax.ShapeDtypeStruct((2, 2, 1, W), f32),
-            jax.ShapeDtypeStruct((2, 1, 128), f32),
+            V((2, 8, W), f32),
+            V((2, 2, 1, W), f32),
+            V((2, 1, 128), f32),
+            V((2, 8, W), f32),
         ),
-        in_specs=[anywhere] * 10,
-        out_specs=(vmem, vmem, vmem),
+        in_specs=[anywhere] * 12,
+        out_specs=(vmem, vmem, vmem, vmem),
         scratch_shapes=[
             V((2, 2, n // 2, d), bf16),
             V((2, d, rank), bf16),
+            V((2, d, rank), bf16),
+            V((n, rank), bf16),
             V((2, n, W), bf16),
             V((2, NG, nx * GR, W), f32),
             V((NG, nx * GR, W), f32),
@@ -408,12 +409,11 @@
             V((2, 2, 1, W), f32),
             V((2, 1, W), f32),
             V((2, 1, W), f32),
-            V((ny, 1, 128), f32),
-            V((NP, 1, 128), f32),
-            V((4 * nx, 1, 128), f32),
+            V((4 * nx * ny, 1, 128), f32),
             V((2, 8, W), f32),
+            V((NG, 16, nx * GR), bf16),
             dma((2, 4)),
-            dma((4,)),
+            dma((6,)),
             dma((NG + 3,)),
             dma((NG + 3,)),
             dma((1,)),
@@ -425,21 +425,22 @@
             dma((NG,)),
             dma((1,)),
             dma((NG,)),
-            dma((3,)),
-            dma((3,)),
+            dma((1,)),
+            dma((1,)),
             pltpu.SemaphoreType.REGULAR((2,)),
         ],
         compiler_params=pltpu.CompilerParams(collective_id=0, has_side_effects=True),
         name="exchange",
-    )(saved, unit, gated, mixer, left, right, m0, m1, s0, s1)
+    )(saved, unit, gated, mixer, left, right, m0, m1, s0, s1, mi, mo.T)
     row = jax.ShapeDtypeStruct((1, W), f32)
     wide = jax.ShapeDtypeStruct((8, W), f32)
     short = jax.ShapeDtypeStruct((8, W), bf16)
     outs = pl.pallas_call(
         functools.partial(finish, entries),
         out_shape=(row, row, row, row, wide, wide, wide, wide, short, short),
+        in_specs=[vmem] * 4,
         name="finish",
-    )(step, fs, q, mi, mo.T)
+    )(*(pltpu.with_memory_space_constraint(v, pltpu.VMEM) for v in (step, fs, q, old)))
     return tuple(out.T if k in (5, 7, 9) else out for k, out in enumerate(outs))
 
 

time: 70.4 us -> 67.6 us (0.960)
  Pallas kernels: 69.6 us -> 66.8 us
    pallas_call x1, Pallas kernels: 68 us -> 66.1 us  [shards(): pl.pallas_call(functools.partial(exchange, nz, nx, ny), out_shape=(V((2,...]
    pallas_call x1, Pallas kernels: 1.55 us -> 0.73 us  [shards(): pl.pallas_call(functools.partial(finish, entries), out_shape=(row, row, r...]
where the time goes in v3:
time: 67.6 us; the launch traced here: 67.5 us
  Pallas kernels  66.8 us (99%)
    pallas_call x1, Pallas kernels, shards(): pl.pallas_call(functools.partial(exchange, nz, nx, ny), out_shape=(V((2,...  66.1 us

profile of v3, /device:TPU:1, one launch (start us, length us, event | category | flops | bytes accessed | tf_op | source)
XLA Modules:
  0.0 67.5 jit_solution(16354713334385578454)
XLA Ops:
  0.6 66.1 %exchange.1 = (f32[2,8,640]{2,1,0:T(8,128)S(1)}, f32[2,2,1,640]{3,2,1,0:T(1,128)S(1)}, f32[2,1,128]{2,1,0:T(1,128)S(1)}, f32[2,8,640]{2,1,0:T(8,128)S(1)}) custom-call(bf16[512,2048]{1,0:T(8,128)(2,1)} %a0.1, bf16[512,640]{1,0:T(8,128)(2,1)} %u0.1, bf16[512,640]{1,0:T(8,128)(2,1)} %u1_.1, bf16[512,2048]{1,0:T(8,128)(2,1)} %a1.1, bf16[2048,256]{1,0:T(8,128)(2,1)} %l0.1, ...), custom_call_target="tpu_custom_call" | custom-call | tf_op jit(solution)/shard_map/exchange/pallas_call | solution.py:383
  66.7 0.7 %finish.1 = (f32[1,640]{1,0:T(1,128)}, f32[1,640]{1,0:T(1,128)}, f32[1,640]{1,0:T(1,128)}, f32[1,640]{1,0:T(1,128)}, f32[8,640]{1,0:T(8,128)}, /*index=5*/f32[8,...) custom-call(f32[2,8,640]{2,1,0:T(8,128)S(1)} %get-tuple-element.24.step, ...), custom_call_target="tpu_custom_call" | custom-call | tf_op jit(solution)/shard_map/finish/pallas_call | solution.py:438

commit v4 on v3

--- a/solution.py
+++ b/solution.py
@@ -265,10 +265,14 @@
                 ).wait_recv()
         for e in range(E):
             piece = ZG[g * E + e]
-            HX[g, x, b, 2 * e : 2 * e + 2] = piece
             piece = piece * piece
             for k in range(0, W, 128):
                 squares = squares + piece[:, k : k + 128]
+        if g == 0:
+            QP[0] = jnp.sum(squares, axis=0, keepdims=True)
+            tell()
+        for e in range(E):
+            HX[g, x, b, 2 * e : 2 * e + 2] = ZG[g * E + e]
         remote(HX.at[g, x, b], HX.at[g, x, b], p_send.at[1], p_recv.at[NG + g], fs_0=twin).start()
         to_x(g, b)
         if g == 0:
@@ -277,8 +281,6 @@
                 remote(
                     HX.at[g, x, b], HX.at[g, x, b], h_send.at[0], h_recv.at[g], fs_0=twin, fs_1=t
                 ).start()
-            QP[0] = jnp.sum(squares, axis=0, keepdims=True)
-            tell()
         return squares
 
     crowd = 4 * nx * ny

time: 67.6 us -> 67.1 us (level)
  no operation moved by 1% of the time
where the time goes in v4:
time: 67.1 us; the launch traced here: 66.8 us
  Pallas kernels  66.2 us (99%)
    pallas_call x1, Pallas kernels, shards(): pl.pallas_call(functools.partial(exchange, nz, nx, ny), out_shape=(V((2,...  65.5 us

profile of v4, /device:TPU:1, one launch (start us, length us, event | category | flops | bytes accessed | tf_op | source)
XLA Modules:
  0.0 66.8 jit_solution(6726490003708566899)
XLA Ops:
  0.6 65.5 %exchange.1 = (f32[2,8,640]{2,1,0:T(8,128)S(1)}, f32[2,2,1,640]{3,2,1,0:T(1,128)S(1)}, f32[2,1,128]{2,1,0:T(1,128)S(1)}, f32[2,8,640]{2,1,0:T(8,128)S(1)}) custom-call(bf16[512,2048]{1,0:T(8,128)(2,1)} %a0.1, bf16[512,640]{1,0:T(8,128)(2,1)} %u0.1, bf16[512,640]{1,0:T(8,128)(2,1)} %u1_.1, bf16[512,2048]{1,0:T(8,128)(2,1)} %a1.1, bf16[2048,256]{1,0:T(8,128)(2,1)} %l0.1, ...), custom_call_target="tpu_custom_call" | custom-call | tf_op jit(solution)/shard_map/exchange/pallas_call | solution.py:385
  66.1 0.7 %finish.1 = (f32[1,640]{1,0:T(1,128)}, f32[1,640]{1,0:T(1,128)}, f32[1,640]{1,0:T(1,128)}, f32[1,640]{1,0:T(1,128)}, f32[8,640]{1,0:T(8,128)}, /*index=5*/f32[8,...) custom-call(f32[2,8,640]{2,1,0:T(8,128)S(1)} %get-tuple-element.24.step, ...), custom_call_target="tpu_custom_call" | custom-call | tf_op jit(solution)/shard_map/finish/pallas_call | solution.py:440
